TPU v7x, 32 devices: a whole 2x2x4 slice. The times are simulated.
32 devices in a mesh: sp: 8 (over z, x), tp: 4 (over y, core).
Axes of the slice: x: 2, y: 2, z: 4, core: 2. Of those that a mesh axis runs over, the one named last changes fastest.
Arguments:
- tokens: bfloat16 [2048, 4096], P('sp', 'tp'), may hold values from -6 to 6
- pre_gain: float32 [4096], replicated, may hold values from 0.1 to 1.9
- rate_factor: float32 [2048], P('sp'), may hold values from 0.5 to 2, as said below
- w_rec_in: bfloat16 [4096, 1024], P(None, 'tp'), may hold values from -0.09375 to 0.09375
- w_rec_gate: bfloat16 [4096, 1024], P(None, 'tp')
- conv_taps: float32 [4, 1024], P(None, 'tp'), may hold values from -3 to 3
- rate_maps: bfloat16 [8, 128, 128], P('tp'), may hold values from -0.5 to 0.5
- input_maps: bfloat16 [8, 128, 128], P('tp'), may hold values from -0.5 to 0.5
- decay_param: float32 [1024], P('tp'), as said below
- w_query: bfloat16 [4096, 1536], P(None, 'tp'), may hold values from -0.09375 to 0.09375
- w_latent: bfloat16 [4096, 512], replicated, may hold values from -0.09375 to 0.09375
- w_rope_key: bfloat16 [4096, 64], replicated, may hold values from -0.09375 to 0.09375
- latent_gain: float32 [512], replicated, may hold values from 0.7 to 100, as said below
- w_expand: bfloat16 [512, 2048], P(None, 'tp')
- rec_gain: float32 [1024], P('tp'), may hold values from 0.1 to 1.9
- att_gain: float32 [1024], P('tp'), may hold values from 0.1 to 1.9
- w_out_rec: bfloat16 [1024, 4096], P('tp'), may hold values from -0.125 to 0.125
- w_out_att: bfloat16 [1024, 4096], P('tp'), may hold values from -0.125 to 0.125
- post_gain: float32 [4096], replicated, may hold values from 0.1 to 1.9
Outputs:
- layer_out: bfloat16 [2048, 4096], P(('sp', 'tp'))
Inputs may be any that keep to these rules, and one draw needn't show every extreme that they name: `rate_factor`: one positive factor for each position. `decay_param`: one parameter for each recurrent channel. `latent_gain`: one positive gain for each latent entry.
All inputs are finite; a program needn't handle non-finite values.
Results may differ from a plain program's by a relative error of at most 0.017.
The roundings to bfloat16 on the way count: a program that leaves them out, or rounds other values in their place, can miss the bound.
Values may be sent and summed in bfloat16 or wider, within the bound.
No kernel may reach another device: no remote copies, remote signals or barrier semaphores. Data moves between devices by JAX's collectives and lax.ppermute only.
A program may use at most 128 MiB of HBM per device.

v0:
```python
import math
import jax
import jax.numpy as jnp
from jax import lax
from jax.sharding import PartitionSpec as P

NOPE = 128
ROPE = 64
VDIM = 128
EPS = 1e-06
RATE_C = 8.0
THETA = 10000.0
span_limit = 2048


def passed_along(block, axis, distance):
    devices = range(lax.axis_size(axis))
    route = [(i - distance, i) for i in devices if i - distance in devices]
    return lax.ppermute(block, axis, route)


def entering(value, axis, join, neutral):
    count, mine = (lax.axis_size(axis), lax.axis_index(axis))
    pieces = jax.tree.map(lambda part: lax.all_gather(part, axis), value)
    subtotal = jax.tree.map(
        lambda part, zero: jnp.full_like(part, 0) + jnp.asarray(zero, part.dtype), value, neutral
    )

    def step(position, subtotal):
        longer = join(subtotal, jax.tree.map(lambda part: part[position], pieces))
        return jax.tree.map(lambda new, old: jnp.where(position < mine, new, old), longer, subtotal)

    return lax.fori_loop(0, count - 1, step, subtotal)


def rms_inverse(values):
    return lax.rsqrt(jnp.mean(values * values, axis=-1, keepdims=True) + EPS)


def rotate(values, cosine, sine_part):
    half_width = values.shape[-1] // 2
    leading = values[..., :half_width]
    trailing = values[..., half_width:]
    return jnp.concatenate(
        [leading * cosine - trailing * sine_part, trailing * cosine + leading * sine_part], axis=-1
    )


def angles(length, offset, span_width):
    frequency = 1.0 / THETA ** (jnp.arange(0, span_width, 2).astype(jnp.float32) / span_width)
    places = (offset + jnp.arange(length)).astype(jnp.float32)
    turned = places[:, None] * frequency[None, :]
    return (jnp.cos(turned), jnp.sin(turned))


def combine_steps(earlier, later):
    return (earlier[0] * later[0], later[0] * earlier[1] + later[1])


def attend_block(state_now, query_nope, query_rope, places, keys_nope, key_rope, values, key_root):
    maxima, totals, accumulated = state_now
    scaling = 1.0 / math.sqrt(query_nope.shape[-1] + query_rope.shape[-1])
    scores = jnp.einsum("qhd,khd->hqk", query_nope, keys_nope, preferred_element_type=jnp.float32)
    scores = scores + jnp.einsum(
        "qhd,kd->hqk", query_rope, key_rope, preferred_element_type=jnp.float32
    )
    scores = scores * scaling
    key_places = key_root + jnp.arange(keys_nope.shape[0])
    visible = key_places[None, :] <= places[:, None]
    scores = jnp.where(visible[None], scores, -jnp.inf)
    largest = jnp.maximum(maxima, jnp.max(scores, axis=-1))
    anchor = jnp.where(largest == -jnp.inf, 0.0, largest)
    weights = jnp.exp(scores - anchor[..., None])
    shrink = jnp.exp(maxima - anchor)
    totals = totals * shrink + jnp.sum(weights, axis=-1)
    accumulated = accumulated * shrink[..., None] + jnp.einsum(
        "hqk,khd->hqd", weights.astype(jnp.bfloat16), values, preferred_element_type=jnp.float32
    )
    return (largest, totals, accumulated)


def shards(
    tokens,
    pre_gain,
    rate_factor,
    w_rec_in,
    w_rec_gate,
    conv_taps,
    rate_maps,
    input_maps,
    decay_param,
    w_query,
    w_latent,
    w_rope_key,
    latent_gain,
    w_expand,
    rec_gain,
    att_gain,
    w_out_rec,
    w_out_att,
    post_gain,
):
    row_count = tokens.shape[0]
    model_width = w_rec_in.shape[0]
    channels = w_rec_in.shape[1]
    heads_here = w_query.shape[1] // (NOPE + ROPE)
    group_size = lax.axis_size("tp")
    first_place = lax.axis_index("sp") * row_count
    places = first_place + jnp.arange(row_count)
    last_place = first_place + row_count - 1
    piece_wide = lax.all_gather(tokens, "tp", axis=1, tiled=True).astype(jnp.float32)
    piece_low = (piece_wide * pre_gain).astype(jnp.bfloat16)

    def accumulate(source, weight):
        return jnp.dot(source, weight, preferred_element_type=jnp.float32)

    squares = jnp.sum(piece_wide * piece_wide, axis=1, keepdims=True)
    sum_input = accumulate(piece_low, w_rec_in)
    sum_gate = accumulate(piece_low, w_rec_gate)
    sum_query = accumulate(piece_low, w_query)
    sum_latent = accumulate(piece_low, w_latent)
    sum_rope = accumulate(piece_low, w_rope_key)
    inverse = lax.rsqrt(squares / model_width + EPS)
    rec_input = (inverse * sum_input).astype(jnp.bfloat16)
    gate_value = inverse * sum_gate
    query_raw = inverse * sum_query
    latent_raw = inverse * sum_latent
    rope_raw = inverse * sum_rope
    taps = conv_taps.shape[0]
    tail_rows = rec_input[row_count - (taps - 1) :]
    before = passed_along(tail_rows, "sp", 1)
    padded = jnp.concatenate([before, rec_input], axis=0)
    convolved = conv_taps[0] * padded[0:row_count].astype(jnp.float32)
    for tap_index in range(1, taps):
        convolved = convolved + conv_taps[tap_index] * padded[
            tap_index : tap_index + row_count
        ].astype(jnp.float32)
    conv_low = convolved.astype(jnp.bfloat16)
    blocks = conv_low.reshape(row_count, rate_maps.shape[0], rate_maps.shape[1])
    rate_gate = jax.nn.sigmoid(
        jnp.einsum("sbi,bij->sbj", blocks, rate_maps, preferred_element_type=jnp.float32)
    ).reshape(row_count, channels)
    entry_gate = jax.nn.sigmoid(
        jnp.einsum("sbi,bij->sbj", blocks, input_maps, preferred_element_type=jnp.float32)
    ).reshape(row_count, channels)
    log_keep = -RATE_C * rate_factor[:, None] * rate_gate * jax.nn.softplus(-decay_param)
    keep_rate = jnp.exp(log_keep)
    driven = jnp.sqrt(-jnp.expm1(2.0 * log_keep)) * entry_gate * convolved
    cum_keep, local_state = lax.associative_scan(combine_steps, (keep_rate, driven), axis=0)
    identity = (jnp.ones((channels,), jnp.float32), jnp.zeros((channels,), jnp.float32))
    chain_keep, carried = entering(
        (cum_keep[row_count - 1], local_state[row_count - 1]), "sp", combine_steps, identity
    )
    state_seq = local_state + cum_keep * carried[None, :]
    rec_out = state_seq * jax.nn.gelu(gate_value)
    rec_squares = jnp.sum(rec_out * rec_out, axis=1, keepdims=True)
    cosine, sine_part = angles(row_count, first_place, ROPE)
    query_heads = query_raw.reshape(row_count, heads_here, NOPE + ROPE)
    query_nope = query_heads[:, :, :NOPE].astype(jnp.bfloat16)
    query_rope = rotate(query_heads[:, :, NOPE:], cosine[:, None, :], sine_part[:, None, :]).astype(
        jnp.bfloat16
    )
    own_latent = (latent_raw * rms_inverse(latent_raw) * latent_gain).astype(jnp.bfloat16)
    rope_key = rotate(rope_raw, cosine, sine_part).astype(jnp.bfloat16)
    start_state = (
        jnp.full((heads_here, row_count), -jnp.inf, jnp.float32),
        jnp.zeros((heads_here, row_count), jnp.float32),
        jnp.zeros((heads_here, row_count, VDIM), jnp.float32),
    )
    expanded_local = jnp.dot(own_latent, w_expand, preferred_element_type=jnp.float32).astype(
        jnp.bfloat16
    )
    key_source = lax.all_gather(expanded_local, "sp", axis=0, tiled=True)
    rope_source = lax.all_gather(rope_key, "sp", axis=0, tiled=True)
    total_rows = key_source.shape[0]
    key_span = math.gcd(total_rows, span_limit)

    def one_span(span_index, state_inner):
        key_root = span_index * key_span

        def compute(state_deep):
            source_rows = lax.dynamic_slice_in_dim(key_source, span_index * key_span, key_span, 0)
            rope_rows = lax.dynamic_slice_in_dim(rope_source, span_index * key_span, key_span, 0)
            expanded = source_rows
            expanded = expanded.reshape(key_span, heads_here, NOPE + VDIM)
            return attend_block(
                state_deep,
                query_nope,
                query_rope,
                places,
                expanded[:, :, :NOPE],
                rope_rows,
                expanded[:, :, NOPE:],
                key_root,
            )

        def keep_state(state_deep):
            return state_deep

        return lax.cond(key_root <= last_place, compute, keep_state, state_inner)

    maxima, totals, accumulated = lax.fori_loop(0, total_rows // key_span, one_span, start_state)
    att_out = (
        (accumulated / totals[..., None]).transpose(1, 0, 2).reshape(row_count, heads_here * VDIM)
    )
    att_squares = jnp.sum(att_out * att_out, axis=1, keepdims=True)
    rec_total, att_total = lax.psum((rec_squares, att_squares), "tp")
    rec_norm = (rec_out * lax.rsqrt(rec_total / (channels * group_size) + EPS) * rec_gain).astype(
        jnp.bfloat16
    )
    att_norm = (
        att_out * lax.rsqrt(att_total / (heads_here * VDIM * group_size) + EPS) * att_gain
    ).astype(jnp.bfloat16)
    mixed_sum = lax.psum_scatter(
        (
            jnp.dot(rec_norm, w_out_rec, preferred_element_type=jnp.float32)
            + jnp.dot(att_norm, w_out_att, preferred_element_type=jnp.float32)
        ).astype(jnp.bfloat16),
        "tp",
        scatter_dimension=0,
        tiled=True,
    ).astype(jnp.float32)
    return (mixed_sum * rms_inverse(mixed_sum) * post_gain).astype(jnp.bfloat16)


def solution(mesh):
    placed = (
        P("sp", "tp"),
        P(),
        P("sp"),
        P(None, "tp"),
        P(None, "tp"),
        P(None, "tp"),
        P("tp", None, None),
        P("tp", None, None),
        P("tp"),
        P(None, "tp"),
        P(),
        P(),
        P(),
        P(None, "tp"),
        P("tp"),
        P("tp"),
        P("tp", None),
        P("tp", None),
        P(),
    )
    return jax.shard_map(
        shards, mesh=mesh, in_specs=placed, out_specs=P(("sp", "tp"), None), check_vma=False
    )
```

profile of v0, /device:TPU:0, one launch (start us, length us, event | category | flops | bytes accessed | tf_op | source)
XLA Modules:
  0.0 334.9 jit_solution(9606723761074546730)
XLA Ops:
  9.8 1.4 fusion.71
  11.2 23.0 %all-gather.5.cloned.1.call-done = bf16[256,4096]{1,0:T(8,128)(2,1)} async-done(((bf16[256,1024]{1,0:T(8,128)(2,1)}), bf16[256,4096]{1,0:T(8,128)(2,1)}) %all-gather.5.cloned.1.call-update) | async-done | bytes 2097168 | tf_op jit(solution)/shard_map/all_gather | solution.py:111
  34.2 2.2 fusion.15
  36.5 2.5 fusion.23
  39.6 4.1 %collective-permute-start = (bf16[3,256]{1,0:T(4,128)(2,1)}, bf16[3,256]{1,0:T(4,128)(2,1)}, u32[]{:S(2)}, u32[]{:S(2)}) collective-permute-start(bf16[3,256]{1,0:T(4,128)(2,1)} %slice.384), channel_id=1, source_target_pairs={{0,4},{4,8},{8,12},{12,16},{16,20},{20,24},{24,28},{1,5},{5,9},{9,... | collective-permute-start | bytes 4616 | tf_op jit(solution)/shard_map/ppermute | solution.py:19
  43.7 1.4 multiply_reduce_fusion
  46.3 3.6 %convolution_multiply_fusion.1 = f32[256,384]{1,0:T(8,128)} fusion(bf16[4096,384]{1,0:T(8,128)(2,1)S(1)} %copy-done, bf16[256,4096]{1,0:T(8,128)(2,1)} %all-gather.5.cloned.1.call-done, f32[4096]{0:T(1024)} %param.24, f32[256]{0:T(256)} %copy-done.20), kind=kOutput, calls=%fused_computation.32 | convolution fusion | flops 808550400 | bytes 5653504 | tf_op jit(solution)/shard_map/dot_general | solution.py:115
  49.9 1.9 copy.55
  51.8 2.6 convolution_multiply_fusion.4
  54.6 33.6 %all_gather.19 = bf16[2048,64]{0,1:T(8,128)(2,1)} all-gather(bf16[256,64]{0,1:T(8,128)(2,1)S(1)} %pad_maximum_fusion.8), channel_id=1, replica_groups=mesh['sp'=8,'tp'=4] {'sp'}, dimensions={0}, use_global_device_ids=true | all-gather | bytes 294912 | tf_op jit(solution)/shard_map/all_gather | solution.py:174
  89.8 1.6 convert_bitcast_fusion
  93.1 1.8 copy.64
  94.9 1.9 fusion.22
  96.7 1.8 copy.63
  98.5 2.2 multiply_multiply_fusion.1
  100.7 1.6 slice.303
  102.3 1.6 slice.302
  103.9 1.6 slice.301
  105.5 1.6 slice.305
  107.1 1.8 multiply_add_fusion.2
  110.1 1.5 slice.306
  111.7 1.5 slice.307
  113.8 1.5 slice.311
  115.4 1.6 multiply_add_fusion.3
  117.0 1.4 slice.315
  118.4 1.4 slice.314
  119.8 1.4 slice.313
  121.3 1.4 slice.317
  122.7 1.4 multiply_add_fusion.4
  163.2 1.4 slice.353
  164.7 1.4 slice.312
  171.1 1.6 slice.357
  172.7 1.6 slice.300
  191.6 1.4 add.362
  193.0 1.4 fusion.61
  196.5 2.0 pad.125
  199.9 2.0 pad.124
  202.0 1.5 add.363
  204.1 1.6 fusion.60
  207.9 2.2 pad.127
  210.1 1.6 add.364
  211.7 2.3 pad.129
  214.0 2.2 pad.111
  216.2 1.5 pad_maximum_fusion.3
  217.6 2.1 pad.110
  219.8 1.6 add.355
  221.4 1.9 fusion.55
  223.3 1.4 pad.128
  225.5 17.7 %all-gather = f32[8,1,256]{2,1,0:T(1,128)S(1)} all-gather(f32[1,1,256]{2,1,0:T(1,128)S(1)} %add_bitcast_fusion.1), channel_id=1, replica_groups=mesh['sp'=8,'tp'=4] {'sp'}, dimensions={0}, use_global_device_ids=true | all-gather | bytes 9216 | tf_op jit(solution)/shard_map/all_gather | solution.py:24
  243.2 2.3 pad.113
  246.5 1.5 pad.112
  248.7 17.0 %all-gather.1 = f32[8,1,256]{2,1,0:T(1,128)S(1)} all-gather(f32[1,1,256]{2,1,0:T(1,128)S(1)} %add_bitcast_fusion), channel_id=1, replica_groups=mesh['sp'=8,'tp'=4] {'sp'}, dimensions={0}, use_global_device_ids=true | all-gather | bytes 9216 | tf_op jit(solution)/shard_map/all_gather | solution.py:24
  266.1 4.0 %multiply_reduce_fusion.1 = (f32[256]{0:T(256)S(1)}, f32[256,256]{1,0:T(8,128)}) fusion(bf16[4096,256]{1,0:T(8,128)(2,1)} %param.27, bf16[256,4096]{1,0:T(8,128)(2,1)} %all-gather.5.cloned.1.call-done, f32[4096]{0:T(1024)} %param.24, f32[256]{0:T(256)} %copy-done.20, f32[256]{0:T(256)S(1)} %get-tuple-element.224, f32[256,256]{1,0:T(8,128)} %pad.128, ...), kind=kOutput, calls=%fused_computation.67 | convolution fusion | flops 541064960 | bytes 5524480 | tf_op jit(solution)/shard_map/dot_general | solution.py:115
  270.1 14.6 %conditional.1 = (f32[2,256]{1,0:T(2,128)S(1)}, f32[2,256,128]{1,2,0:T(8,128)}) conditional(s32[]{:T(128)} %convert_element_type.81, (f32[2,256]{1,0:T(2,128)S(1)}, f32[2,256,128]{2,1,0:T(8,128)S(1)}) %tuple.113, (s32[]{:T(128)}, s32[256]{0:T(256)S(1)}, bf16[2048,512]{1,0:T(8,128)(2,1)}, f32[256,2,192]{0,2,1:T(8,128)}, bf16[2048,64]{0,1:T(8,128)(2,1)}, ...), branch_computations={%region_6.7_spmd, %region_7.10_spmd} | conditional | flops 680135424 | bytes 39873612 | solution.py:200
  270.1 4.0 %copy.56 = bf16[2048,512]{0,1:T(8,128)(2,1)} copy(bf16[2048,512]{1,0:T(8,128)(2,1)} %get-tuple-element.265) | data formatting | bytes 4194304 | tf_op jit(solution)/shard_map
  274.1 1.9 copy.57
  276.0 2.0 fusion.11
  281.3 1.6 fusion.7
  282.9 1.8 copy.66
  285.7 5.7 %all-reduce.32 = (f32[256,1]{0,1:T(1,128)S(1)}, f32[256,1]{0,1:T(1,128)S(1)}) all-reduce(f32[256,1]{0,1:T(1,128)S(1)} %bitcast.90, f32[256,1]{0,1:T(1,128)S(1)} %bitcast.84), channel_id=1, replica_groups=mesh['sp'=8,'tp'=4] {'tp'}, use_global_device_ids=true, to_apply=%region_4.5 | all-reduce | flops 512 | bytes 4096 | tf_op jit(solution)/shard_map/psum | solution.py:207
  291.5 2.6 fusion.52
  294.1 2.1 fusion.14
  296.2 28.9 %reduce-scatter.2.cloned.1.call-done = bf16[64,4096]{1,0:T(8,128)(2,1)} async-done(((bf16[256,4096]{1,0:T(8,128)(2,1)}), bf16[64,4096]{1,0:T(8,128)(2,1)}) %reduce-scatter.2.cloned.1.call-update) | async-done | bytes 524304 | tf_op jit(solution)/shard_map/reduce_scatter | solution.py:214
  326.4 2.0 fusion.31
  (193 shorter events, 86.4 us)
Async XLA Ops:
  6.5 39.7 %copy-start = (bf16[4096,384]{1,0:T(8,128)(2,1)S(1)}, bf16[4096,384]{1,0:T(8,128)(2,1)}, u32[]{:S(2)}) copy-start(bf16[4096,384]{1,0:T(8,128)(2,1)} %param.32) | copy-start | bytes 9437188
  6.5 27.7 %all-gather.5.cloned.1.call-start = ((), (), s32[]{:S(2)}) async-start(), calls=%async_computation.1 | async-start | bytes 2621440 | tf_op jit(solution)/shard_map/all_gather | solution.py:111
  7.3 262.8 %all-gather.7.cloned.1.call-start = ((), (), s32[]{:S(2)}) async-start(), calls=%async_computation.2 | async-start | bytes 2359296 | tf_op jit(solution)/shard_map/all_gather | solution.py:173
  34.2 2.2 copy-start.2
  36.5 7.2 %copy-start.20 = (f32[256]{0:T(256)}, f32[256]{0:T(256)S(1)}, u32[]{:S(2)}) copy-start(f32[256]{0:T(256)S(1)} %add_rsqrt_fusion.3) | copy-start | bytes 3076
  36.5 7.2 %copy-start.22 = (bf16[4096,512]{1,0:T(8,128)(2,1)S(1)}, bf16[4096,512]{1,0:T(8,128)(2,1)}, u32[]{:S(2)}) copy-start(bf16[4096,512]{1,0:T(8,128)(2,1)} %param.33) | copy-start | bytes 12582916
  36.5 7.2 %copy-start.24 = (f32[4096]{0:T(1024)S(1)}, f32[4096]{0:T(1024)}, u32[]{:S(2)}) copy-start(f32[4096]{0:T(1024)} %param.24) | copy-start | bytes 49156
  39.6 5.5 %copy-start.5 = (bf16[512,512]{1,0:T(8,128)(2,1)S(1)}, bf16[512,512]{1,0:T(8,128)(2,1)}, u32[]{:S(2)}) copy-start(bf16[512,512]{1,0:T(8,128)(2,1)} %param.36) | copy-start | bytes 1572868
  39.6 5.5 %copy-start.17 = (f32[512]{0:T(512)S(1)}, f32[512]{0:T(512)}, u32[]{:S(2)}) copy-start(f32[512]{0:T(512)} %param.35) | copy-start | bytes 6148
  39.6 50.2 %collective-permute-start = (bf16[3,256]{1,0:T(4,128)(2,1)}, bf16[3,256]{1,0:T(4,128)(2,1)}, u32[]{:S(2)}, u32[]{:S(2)}) collective-permute-start(bf16[3,256]{1,0:T(4,128)(2,1)} %slice.384), channel_id=1, source_target_pairs={{0,4},{4,8},{8,12},{12,16},{16,20},{20,24},{24,28},{1,5},{5,9},{9,... | collective-permute-start | bytes 4616 | tf_op jit(solution)/shard_map/ppermute | solution.py:19
  46.2 278.9 %reduce-scatter.2.cloned.1.call-start = ((), (), s32[]{:S(2)}) async-start(), calls=%async_computation.3 | async-start | bytes 2621440 | tf_op jit(solution)/shard_map/reduce_scatter | solution.py:214
  51.8 2.6 copy-start.19
  51.8 2.6 copy-start.21
  51.8 38.0 %copy-start.15 = (f32[1,256]{1,0:T(1,128)S(1)}, f32[1,256]{1,0:T(1,128)}, u32[]{:S(2)}) copy-start(f32[1,256]{1,0:T(1,128)} %get-tuple-element.332) | copy-start | bytes 3076
  51.8 38.0 %copy-start.16 = (f32[1,256]{1,0:T(1,128)S(1)}, f32[1,256]{1,0:T(1,128)}, u32[]{:S(2)}) copy-start(f32[1,256]{1,0:T(1,128)} %get-tuple-element.333) | copy-start | bytes 3076
  51.8 40.3 %copy-start.23 = (bf16[2,128,128]{2,1,0:T(8,128)(2,1)S(1)}, bf16[2,128,128]{2,1,0:T(8,128)(2,1)}, u32[]{:S(2)}) copy-start(bf16[2,128,128]{2,1,0:T(8,128)(2,1)} %param.30) | copy-start | bytes 196612
  91.4 0.7 copy-start.7
  191.6 24.5 %copy-start.14 = (f32[1,256]{1,0:T(1,128)S(1)}, f32[1,256]{1,0:T(1,128)}, u32[]{:S(2)}) copy-start(f32[1,256]{1,0:T(1,128)} %slice.390) | copy-start | bytes 3076
  202.0 21.3 %copy-start.13 = (f32[1,256]{1,0:T(1,128)S(1)}, f32[1,256]{1,0:T(1,128)}, u32[]{:S(2)}) copy-start(f32[1,256]{1,0:T(1,128)} %slice.415) | copy-start | bytes 3076
  207.0 38.6 %copy-start.12 = (f32[1,256]{1,0:T(1,128)S(1)}, f32[1,256]{1,0:T(1,128)}, u32[]{:S(2)}) copy-start(f32[1,256]{1,0:T(1,128)} %slice.389) | copy-start | bytes 3076
  211.7 54.0 %copy-start.8 = (f32[256]{0:T(256)S(1)}, f32[256]{0:T(256)}, u32[]{:S(2)}) copy-start(f32[256]{0:T(256)} %custom-call) | copy-start | bytes 3076
  266.1 4.0 %copy-start.6 = (bf16[256,2,64]{0,2,1:T(8,128)(2,1)S(1)}, bf16[256,2,64]{0,2,1:T(8,128)(2,1)}, u32[]{:S(2)}) copy-start(bf16[256,2,64]{0,2,1:T(8,128)(2,1)} %pad_maximum_fusion.5) | copy-start | bytes 196612
  266.1 4.0 %copy-start.9 = (f32[2,256]{1,0:T(2,128)S(1)}, f32[2,256]{1,0:T(2,128)}, u32[]{:S(2)}) copy-start(f32[2,256]{1,0:T(2,128)} %broadcast_in_dim.63) | copy-start | bytes 6148
  270.1 21.3 %copy-start.18 = (f32[256]{0:T(256)S(1)}, f32[256]{0:T(256)}, u32[]{:S(2)}) copy-start(f32[256]{0:T(256)} %param.38) | copy-start | bytes 3076
  270.1 21.4 %copy-start.11 = (f32[256]{0:T(256)S(1)}, f32[256]{0:T(256)}, u32[]{:S(2)}) copy-start(f32[256]{0:T(256)} %param.37) | copy-start | bytes 3076
  276.0 2.4 copy-start.4
  279.7 1.6 copy-start.1
  291.5 2.6 copy-start.3
  296.2 30.2 %copy-start.10 = (f32[4096]{0:T(1024)S(1)}, f32[4096]{0:T(1024)}, u32[]{:S(2)}) copy-start(f32[4096]{0:T(1024)} %param.41) | copy-start | bytes 49156
Sparse Core Ops, SparseCore 0:
  8.9 25.2 all-gather.4
  46.3 49.1 all-gather.6
  296.4 28.7 reduce-scatter.1
where the time goes:
time: 339 us; the launch traced here: 335 us
  local copies, waits for them, and re-layouts  107 us (32%)
  blocking collectives  74 us (22%)
  other arithmetic  55.4 us (16%)
  waiting for transfers between devices  52.6 us (16%)
  matrix products  27.6 us (8%)
  between operations  13.5 us (4%)
  starting transfers between devices  4.15 us (1%)
    slice x52, local copies, waits for them, and re-layouts, shards(): lax.associative_scan(combine_steps, (keep_rate, driven), axis=0)  64.7 us
    all_gather x2, blocking collectives, entering(): pieces = jax.tree.map(lambda part: lax.all_gather(part, axis), value)  34.8 us
    all_gather x1, blocking collectives, shards(): rope_source = lax.all_gather(rope_key, 'sp', axis=0, tiled=True)  33.6 us
    reduce_scatter x1, waiting for transfers between devices, shards(): lax.psum_scatter((jnp.dot(rec_norm, w_out_rec, preferred_element_type=jnp...  28.9 us
    pad x28, local copies, waits for them, and re-layouts, shards(): lax.associative_scan(combine_steps, (keep_rate, driven), axis=0)  25.2 us
    all_gather x1, waiting for transfers between devices, shards(): lax.all_gather(tokens, 'tp', axis=1, tiled=True).astype(jnp.float32)  23 us
    add x13, other arithmetic, combine_steps(): return (earlier[0] * later[0], later[0] * earlier[1] + later[1])  17.2 us
    dot_general x5, matrix products, accumulate(): return jnp.dot(source, weight, preferred_element_type=jnp.float32)  14.1 us
  transfers between devices with their start and end apart: 4, of which 2 were waited for; matrix products, arithmetic and copies ran while one was open for 48% of the time, Pallas kernels for 0%

commit v1 on v0

--- a/solution.py
+++ b/solution.py
@@ -108,7 +108,7 @@
     first_place = lax.axis_index("sp") * row_count
     places = first_place + jnp.arange(row_count)
     last_place = first_place + row_count - 1
-    piece_wide = lax.all_gather(tokens, "tp", axis=1, tiled=True).astype(jnp.float32)
+    piece_wide = jnp.concatenate(lax.all_gather(tokens, "tp"), axis=1).astype(jnp.float32)
     piece_low = (piece_wide * pre_gain).astype(jnp.bfloat16)
 
     def accumulate(source, weight):

time: 339 us -> 289 us (0.85)
  local copies, waits for them, and re-layouts: 107 us -> 71.5 us
  other arithmetic: 55.4 us -> 46.7 us
    slice x52, local copies, waits for them, and re-layouts: 64.7 us -> 25.5 us  [shards(): lax.associative_scan(combine_steps, (keep_rate, driven), axis=0)]
    add x13, other arithmetic: 17.2 us -> 8.49 us  [combine_steps(): return (earlier[0] * later[0], later[0] * earlier[1] + later[1])]
    convert_element_type x0 -> x1, local copies, waits for them, and re-layouts: none -> 5.38 us  [shards(): jnp.concatenate(lax.all_gather(tokens, 'tp'), axis=1).astype(jnp.float32)]
    pad x28, local copies, waits for them, and re-layouts: 25.2 us -> 19.9 us  [shards(): lax.associative_scan(combine_steps, (keep_rate, driven), axis=0)]
    convert_element_type x0 -> x2, other arithmetic: none -> 5.09 us  [the longest x1 2.64 us: shards(): piece_low = (piece_wide * pre_gain).astype(jnp.bfloat16)]
    dot_general x5, matrix products: 14.1 us -> 9.36 us  [accumulate(): return jnp.dot(source, weight, preferred_element_type=jnp.float32)]
    concatenate x14, other arithmetic: 11.1 us -> 7.12 us  [shards(): lax.associative_scan(combine_steps, (keep_rate, driven), axis=0)]
  transfers between devices with their start and end apart: 4 -> 4, of which waited for: 2 -> 2; matrix products, arithmetic and copies ran while one was open for 48% -> 35% of each run, Pallas kernels for 0% -> 0%
where the time goes in v1:
time: 289 us; the launch traced here: 287 us
  blocking collectives  73.4 us (25%)
  local copies, waits for them, and re-layouts  71.5 us (25%)
  waiting for transfers between devices  52.4 us (18%)
  other arithmetic  46.7 us (16%)
  matrix products  25 us (9%)
  between operations  13.6 us (5%)
  starting transfers between devices  4.03 us (1%)
    all_gather x2, blocking collectives, entering(): pieces = jax.tree.map(lambda part: lax.all_gather(part, axis), value)  34.8 us
    all_gather x1, blocking collectives, shards(): rope_source = lax.all_gather(rope_key, 'sp', axis=0, tiled=True)  32.8 us
    reduce_scatter x1, waiting for transfers between devices, shards(): lax.psum_scatter((jnp.dot(rec_norm, w_out_rec, preferred_element_type=jnp...  28.6 us
    slice x52, local copies, waits for them, and re-layouts, shards(): lax.associative_scan(combine_steps, (keep_rate, driven), axis=0)  25.5 us
    all_gather x1, waiting for transfers between devices, shards(): lax.all_gather(tokens, 'tp')  23 us
    pad x28, local copies, waits for them, and re-layouts, shards(): lax.associative_scan(combine_steps, (keep_rate, driven), axis=0)  19.9 us
    dot_general x5, matrix products, accumulate(): return jnp.dot(source, weight, preferred_element_type=jnp.float32)  9.36 us
    add x13, other arithmetic, combine_steps(): return (earlier[0] * later[0], later[0] * earlier[1] + later[1])  8.49 us
  transfers between devices with their start and end apart: 4, of which 2 were waited for; matrix products, arithmetic and copies ran while one was open for 35% of the time, Pallas kernels for 0%

profile of v1, /device:TPU:0, one launch (start us, length us, event | category | flops | bytes accessed | tf_op | source)
XLA Modules:
  0.0 286.9 jit_solution(11076887305075248492)
XLA Ops:
  9.8 1.4 fusion.62
  11.2 23.0 %all-gather.8.cloned.1.call-done = bf16[1024,1024]{1,0:T(8,128)(2,1)} async-done(((bf16[256,1024]{1,0:T(8,128)(2,1)}), bf16[1024,1024]{1,0:T(8,128)(2,1)}) %all-gather.8.cloned.1.call-update) | async-done | bytes 2097168 | tf_op jit(solution)/shard_map/all_gather | solution.py:111
  34.2 2.2 fusion.15
  36.5 2.4 convert_bitcast_fusion
  38.9 5.4 %copy.63 = f32[256,4,1024]{0,2,1:T(8,128)} copy(f32[256,4,1024]{2,0,1:T(8,128)} %convert_bitcast_fusion) | data formatting | bytes 8388608 | tf_op jit(solution)/shard_map/convert_element_type | solution.py:111
  44.3 2.6 fusion.16
  47.5 1.9 copy-done.27
  50.7 3.9 %collective-permute-start = (bf16[3,256]{1,0:T(4,128)(2,1)}, bf16[3,256]{1,0:T(4,128)(2,1)}, u32[]{:S(2)}, u32[]{:S(2)}) collective-permute-start(bf16[3,256]{1,0:T(4,128)(2,1)} %slice.384), channel_id=1, source_target_pairs={{0,4},{4,8},{8,12},{12,16},{16,20},{20,24},{24,28},{1,5},{5,9},{9,... | collective-permute-start | bytes 4616 | tf_op jit(solution)/shard_map/ppermute | solution.py:19
  55.5 32.8 %all_gather.23 = bf16[2048,64]{0,1:T(8,128)(2,1)} all-gather(bf16[256,64]{0,1:T(8,128)(2,1)S(1)} %pad_maximum_fusion.8), channel_id=1, replica_groups=mesh['sp'=8,'tp'=4] {'sp'}, dimensions={0}, use_global_device_ids=true | all-gather | bytes 294912 | tf_op jit(solution)/shard_map/all_gather | solution.py:174
  88.3 2.1 convolution_multiply_fusion.1
  90.5 2.1 multiply_reduce_fusion
  93.1 1.9 copy.71
  95.0 2.3 convolution_convert_fusion
  98.9 1.6 convert_bitcast_fusion.1
  101.2 1.8 fusion.19
  103.0 1.8 copy.80
  104.8 1.9 fusion.22
  106.7 1.8 copy.79
  108.5 2.1 multiply_multiply_fusion.1
  111.8 1.6 slice.357
  113.4 1.6 slice.303
  115.0 1.6 slice.302
  116.6 1.2 slice.415
  117.9 1.6 slice.305
  119.5 1.6 slice.301
  121.1 1.7 slice.300
  125.1 1.5 slice.355
  126.6 1.5 slice.309
  128.2 1.5 slice.308
  144.2 1.4 fusion.52
  146.2 1.4 pad_maximum_fusion.6
  148.4 2.0 pad.109
  150.4 2.0 pad.125
  152.4 1.5 add.363
  153.9 1.5 add.353
  155.3 1.6 fusion.51
  156.9 1.3 pad_maximum_fusion.4
  159.1 1.5 pad_maximum_fusion.3
  160.5 2.2 pad.110
  162.7 2.2 pad.111
  164.9 2.2 pad.127
  167.1 1.6 add.364
  168.6 1.6 add.355
  170.3 1.9 fusion.46
  172.1 1.5 pad.128
  174.5 1.5 pad.112
  176.0 2.3 pad.113
  179.1 17.7 %all-gather.2 = f32[8,1,256]{2,1,0:T(1,128)S(1)} all-gather(f32[1,1,256]{2,1,0:T(1,128)S(1)} %add_bitcast_fusion), channel_id=1, replica_groups=mesh['sp'=8,'tp'=4] {'sp'}, dimensions={0}, use_global_device_ids=true | all-gather | bytes 9216 | tf_op jit(solution)/shard_map/all_gather | solution.py:24
  196.8 2.3 pad.129
  199.8 17.0 %all-gather.1 = f32[8,1,256]{2,1,0:T(1,128)S(1)} all-gather(f32[1,1,256]{2,1,0:T(1,128)S(1)} %add_bitcast_fusion.1), channel_id=1, replica_groups=mesh['sp'=8,'tp'=4] {'sp'}, dimensions={0}, use_global_device_ids=true | all-gather | bytes 9216 | tf_op jit(solution)/shard_map/all_gather | solution.py:24
  217.3 4.0 %multiply_reduce_fusion.1 = (f32[256]{0:T(256)S(1)}, f32[256,256]{1,0:T(8,128)}) fusion(bf16[256,4096]{0,1:T(8,128)(2,1)} %copy-done.1, bf16[4096,256]{1,0:T(8,128)(2,1)} %param.27, f32[256]{0:T(256)S(1)} %copy-done.17, f32[256]{0:T(256)S(1)} %get-tuple-element.224, f32[256,256]{1,0:T(8,128)} %pad.128, f32[256,256]{1,0:T(8,128)} %pad.129, ...), kind=kOutput, calls=%fused_computation.68 | convolution fusion | flops 537919232 | bytes 5508096 | tf_op jit(solution)/shard_map/dot_general | solution.py:115
  221.3 15.4 %conditional.1 = (f32[2,256]{1,0:T(2,128)S(1)}, f32[2,256,128]{1,2,0:T(8,128)}) conditional(s32[]{:T(128)} %convert_element_type.94, (f32[2,256]{1,0:T(2,128)S(1)}, f32[2,256,128]{2,1,0:T(8,128)S(1)}) %tuple.114, (s32[]{:T(128)}, s32[256]{0:T(256)S(1)}, bf16[2048,512]{1,0:T(8,128)(2,1)}, f32[256,2,192]{0,2,1:T(8,128)}, bf16[2048,64]{0,1:T(8,128)(2,1)}, ...), branch_computations={%region_6.7_spmd, %region_7.10_spmd} | conditional | flops 680135424 | bytes 41970792 | solution.py:200
  221.3 1.9 copy.73
  224.4 3.9 %copy.72 = bf16[2048,512]{0,1:T(8,128)(2,1)} copy(bf16[2048,512]{1,0:T(8,128)(2,1)} %get-tuple-element.273) | data formatting | bytes 4194304 | tf_op jit(solution)/shard_map
  228.3 2.1 fusion.11
  230.4 1.3 fusion.60
  233.3 1.6 fusion.7
  234.9 1.8 copy.82
  237.7 5.9 %all-reduce.32 = (f32[256,1]{0,1:T(1,128)S(1)}, f32[256,1]{0,1:T(1,128)S(1)}) all-reduce(f32[256,1]{0,1:T(1,128)S(1)} %bitcast.105, f32[256,1]{0,1:T(1,128)S(1)} %bitcast.99), channel_id=1, replica_groups=mesh['sp'=8,'tp'=4] {'tp'}, use_global_device_ids=true, to_apply=%region_4.5 | all-reduce | flops 512 | bytes 4096 | tf_op jit(solution)/shard_map/psum | solution.py:207
  243.7 2.6 fusion.43
  246.3 2.1 fusion.14
  248.5 28.6 %reduce-scatter.2.cloned.1.call-done = bf16[64,4096]{1,0:T(8,128)(2,1)} async-done(((bf16[256,4096]{1,0:T(8,128)(2,1)}), bf16[64,4096]{1,0:T(8,128)(2,1)}) %reduce-scatter.2.cloned.1.call-update) | async-done | bytes 524304 | tf_op jit(solution)/shard_map/reduce_scatter | solution.py:214
  277.1 1.2 fusion.24
  278.4 2.0 fusion.26
  (202 shorter events, 35.9 us)
Async XLA Ops:
  6.5 81.7 %copy-start = (bf16[4096,384]{1,0:T(8,128)(2,1)S(1)}, bf16[4096,384]{1,0:T(8,128)(2,1)}, u32[]{:S(2)}) copy-start(bf16[4096,384]{1,0:T(8,128)(2,1)} %param.32) | copy-start | bytes 9437188
  6.5 27.7 %all-gather.8.cloned.1.call-start = ((), (), s32[]{:S(2)}) async-start(), calls=%async_computation.3 | async-start | bytes 2621440 | tf_op jit(solution)/shard_map/all_gather | solution.py:111
  7.3 214.0 %all-gather.6.cloned.1.call-start = ((), (), s32[]{:S(2)}) async-start(), calls=%async_computation.1 | async-start | bytes 2359296 | tf_op jit(solution)/shard_map/all_gather | solution.py:173
  34.2 2.2 copy-start.2
  36.5 53.9 %copy-start.16 = (f32[256]{0:T(256)}, f32[256]{0:T(256)S(1)}, u32[]{:S(2)}) copy-start(f32[256]{0:T(256)S(1)} %add_rsqrt_fusion.3) | copy-start | bytes 3076
  38.9 5.4 %copy-start.14 = (f32[4096]{0:T(1024)S(1)}, f32[4096]{0:T(1024)}, u32[]{:S(2)}) copy-start(f32[4096]{0:T(1024)} %param.24) | copy-start | bytes 49156
  44.3 2.7 copy-start.9
  47.0 43.4 %copy-start.1 = (bf16[256,4096]{0,1:T(8,128)(2,1)}, bf16[256,4096]{0,1:T(8,128)(2,1)S(1)}, u32[]{:S(2)}) copy-start(bf16[256,4096]{0,1:T(8,128)(2,1)S(1)} %fusion.16) | copy-start | bytes 6291460
  47.0 2.4 copy-start.27
  49.3 5.3 %copy-start.24 = (f32[256]{0:T(256)S(1)}, f32[256]{0:T(256)}, u32[]{:S(2)}) copy-start(f32[256]{0:T(256)} %add_convert_fusion.2) | copy-start | bytes 3076
  49.3 5.3 %copy-start.25 = (f32[32]{0:T(128)S(1)}, f32[32]{0:T(128)}, u32[]{:S(2)}) copy-start(f32[32]{0:T(128)} %negate_power_fusion) | copy-start | bytes 388
  50.7 48.2 %collective-permute-start = (bf16[3,256]{1,0:T(4,128)(2,1)}, bf16[3,256]{1,0:T(4,128)(2,1)}, u32[]{:S(2)}, u32[]{:S(2)}) collective-permute-start(bf16[3,256]{1,0:T(4,128)(2,1)} %slice.384), channel_id=1, source_target_pairs={{0,4},{4,8},{8,12},{12,16},{16,20},{20,24},{24,28},{1,5},{5,9},{9,... | collective-permute-start | bytes 4616 | tf_op jit(solution)/shard_map/ppermute | solution.py:19
  88.3 2.2 copy-start.26
  92.5 6.4 %copy-start.22 = (f32[1,256]{1,0:T(1,128)S(1)}, f32[1,256]{1,0:T(1,128)}, u32[]{:S(2)}) copy-start(f32[1,256]{1,0:T(1,128)} %get-tuple-element.339) | copy-start | bytes 3076
  97.3 179.8 %reduce-scatter.2.cloned.1.call-start = ((), (), s32[]{:S(2)}) async-start(), calls=%async_computation.2 | async-start | bytes 2621440 | tf_op jit(solution)/shard_map/reduce_scatter | solution.py:214
  100.6 0.7 copy-start.11
  110.6 0.7 copy-start.6
  123.9 0.7 copy-start.8
  142.9 16.1 %copy-start.21 = (f32[1,256]{1,0:T(1,128)S(1)}, f32[1,256]{1,0:T(1,128)}, u32[]{:S(2)}) copy-start(f32[1,256]{1,0:T(1,128)} %slice.390) | copy-start | bytes 3076
  146.2 25.9 %copy-start.20 = (f32[1,256]{1,0:T(1,128)S(1)}, f32[1,256]{1,0:T(1,128)}, u32[]{:S(2)}) copy-start(f32[1,256]{1,0:T(1,128)} %slice.415) | copy-start | bytes 3076
  153.9 19.8 %copy-start.19 = (f32[1,256]{1,0:T(1,128)S(1)}, f32[1,256]{1,0:T(1,128)}, u32[]{:S(2)}) copy-start(f32[1,256]{1,0:T(1,128)} %slice.389) | copy-start | bytes 3076
  164.9 52.0 %copy-start.12 = (f32[256]{0:T(256)S(1)}, f32[256]{0:T(256)}, u32[]{:S(2)}) copy-start(f32[256]{0:T(256)} %custom-call) | copy-start | bytes 3076
  167.1 50.2 %copy-start.17 = (f32[256]{0:T(256)S(1)}, f32[256]{0:T(256)}, u32[]{:S(2)}) copy-start(f32[256]{0:T(256)} %copy-done.16) | copy-start | bytes 3076
  217.2 4.0 %copy-start.10 = (bf16[256,2,64]{0,2,1:T(8,128)(2,1)S(1)}, bf16[256,2,64]{0,2,1:T(8,128)(2,1)}, u32[]{:S(2)}) copy-start(bf16[256,2,64]{0,2,1:T(8,128)(2,1)} %pad_maximum_fusion.5) | copy-start | bytes 196612
  217.3 4.0 %copy-start.13 = (f32[2,256]{1,0:T(2,128)S(1)}, f32[2,256]{1,0:T(2,128)}, u32[]{:S(2)}) copy-start(f32[2,256]{1,0:T(2,128)} %broadcast_in_dim.63) | copy-start | bytes 6148
  221.3 22.3 %copy-start.23 = (f32[256]{0:T(256)S(1)}, f32[256]{0:T(256)}, u32[]{:S(2)}) copy-start(f32[256]{0:T(256)} %param.38) | copy-start | bytes 3076
  221.3 22.4 %copy-start.18 = (f32[256]{0:T(256)S(1)}, f32[256]{0:T(256)}, u32[]{:S(2)}) copy-start(f32[256]{0:T(256)} %param.37) | copy-start | bytes 3076
  228.3 2.1 copy-start.4
  228.3 2.1 copy-start.7
  231.7 1.6 copy-start.3
  243.7 2.6 copy-start.5
  248.4 29.9 %copy-start.15 = (f32[4096]{0:T(1024)S(1)}, f32[4096]{0:T(1024)}, u32[]{:S(2)}) copy-start(f32[4096]{0:T(1024)} %param.41) | copy-start | bytes 49156
Sparse Core Ops, SparseCore 0:
  8.9 25.2 all-gather.7
  97.5 46.3 all-gather.5
  248.6 28.4 reduce-scatter.1
